TPU v7x, 32 devices: a whole 2x2x4 slice. The times are simulated.
32 devices in a mesh: ep: 16 (over z, y, x), tp: 2 (over core).
Axes of the slice: x: 2, y: 2, z: 4, core: 2. Of those that a mesh axis runs over, the one named last changes fastest.
Arguments:
- tokens: bfloat16 [384, 4096], P('ep'), may hold values from -6 to 6
- in_gain: float32 [4096], replicated, may hold values from 0.1 to 1.9
- routes: int32 [384, 6], P('ep'), may hold values from 0 to 15, all different within a row; in each aligned block of 24 rows (0 to 23, 24 to 47, ...) at most 10 rows name the same one
- gates: float32 [384, 6], P('ep'), may hold values from 0.25 to 1.5
- expert_gate: bfloat16 [16, 512, 4096], P('ep', 'tp'), may hold values from -0.09375 to 0.09375
- expert_up: bfloat16 [16, 512, 4096], P('ep', 'tp'), may hold values from -0.09375 to 0.09375
- expert_down: bfloat16 [16, 512, 4096], P('ep', None, 'tp'), may hold values from -0.25 to 0.25
- shared_gate: bfloat16 [512, 4096], P('tp'), may hold values from -0.09375 to 0.09375
- shared_up: bfloat16 [512, 4096], P('tp'), may hold values from -0.09375 to 0.09375
- shared_down: bfloat16 [512, 4096], P(None, 'tp')
- out_gain: float32 [4096], P('tp'), may hold values from 0.1 to 1.9
Outputs:
- mixed: bfloat16 [384, 4096], P('ep', 'tp')
Inputs may be any that keep to these rules, and one draw needn't show every extreme that they name: `routes`: each row names 6 different experts; among the 24 rows of one index of ep no expert is named more than 10 times, and on some index of ep some expert is named exactly 10 times.
All inputs are finite; a program needn't handle non-finite values.
Results may differ from a plain program's by a relative error of at most 0.0075.
Values may be sent and summed in bfloat16 or wider, within the bound.
A program may use at most 64 MiB of HBM per device.

v0:
```python
import jax
import jax.numpy as jnp
from jax import lax
from jax.sharding import PartitionSpec as P

EPS = 1e-06


def project(rows, weight):
    return lax.dot_general(
        rows, weight, (((1,), (1,)), ((), ())), preferred_element_type=jnp.float32
    )


def on_device(
    tokens,
    in_gain,
    routes,
    gates,
    expert_gate,
    expert_up,
    expert_down,
    shared_gate,
    shared_up,
    shared_down,
    out_gain,
):
    experts = lax.axis_size("ep")
    local_rows = tokens.shape[0]
    model_width = tokens.shape[1]
    top_count = routes.shape[1]
    tokens_f = tokens.astype(jnp.float32)
    normed = (
        tokens_f * lax.rsqrt(jnp.mean(tokens_f * tokens_f, axis=1, keepdims=True) + EPS) * in_gain
    ).astype(jnp.bfloat16)
    shared_hidden = (jax.nn.silu(project(normed, shared_gate)) * project(normed, shared_up)).astype(
        jnp.bfloat16
    )
    w_gate = expert_gate[0]
    w_up = expert_up[0]
    w_down = expert_down[0]
    capacity = min(local_rows, (local_rows * top_count + experts - 1) // experts + 1)
    flat_routes = routes.reshape(-1)
    onehot = (flat_routes[:, None] == jnp.arange(experts, dtype=jnp.int32)[None, :]).astype(
        jnp.int32
    )
    before = jnp.cumsum(onehot, axis=0) - onehot
    slot_index = jnp.sum(before * onehot, axis=1)
    column = (flat_routes * capacity + slot_index).reshape(local_rows, top_count)
    matches = column[:, :, None] == jnp.arange(experts * capacity, dtype=jnp.int32)[None, None, :]
    placing = jnp.any(matches, axis=1).astype(jnp.bfloat16)
    mixing = jnp.sum(jnp.where(matches, gates[:, :, None], 0.0), axis=1)
    buffer = lax.dot_general(
        placing, normed, (((0,), (0,)), ((), ())), preferred_element_type=jnp.float32
    ).astype(jnp.bfloat16)
    arrived = lax.all_to_all(
        buffer.reshape(experts, capacity, model_width),
        "ep",
        split_axis=0,
        concat_axis=0,
        tiled=True,
    )
    token_rows = arrived.reshape(experts * capacity, model_width)
    hidden = (jax.nn.silu(project(token_rows, w_gate)) * project(token_rows, w_up)).astype(
        jnp.bfloat16
    )
    hidden_all = lax.all_gather(hidden, "tp", axis=1, tiled=True)
    shared_all = lax.all_gather(shared_hidden, "tp", axis=1, tiled=True)
    outputs = jnp.dot(hidden_all, w_down, preferred_element_type=jnp.float32).astype(jnp.bfloat16)
    outputs, shared_out = (
        outputs,
        jnp.dot(shared_all, shared_down, preferred_element_type=jnp.float32),
    )
    returned = lax.all_to_all(
        outputs.reshape(experts, capacity, outputs.shape[1]),
        "ep",
        split_axis=0,
        concat_axis=0,
        tiled=True,
    )
    returned = returned.reshape(experts * capacity, outputs.shape[1]).astype(jnp.float32)
    routed = jnp.dot(mixing, returned, precision=lax.Precision.HIGHEST)
    combined = routed + shared_out
    squares_sum = lax.psum(jnp.sum(combined * combined, axis=1), "tp")
    scale = lax.rsqrt(squares_sum / model_width + EPS)
    return (combined * scale[:, None] * out_gain[None, :]).astype(jnp.bfloat16)


def solution(mesh):
    in_specs = (
        P("ep", None),
        P(),
        P("ep", None),
        P("ep", None),
        P("ep", "tp", None),
        P("ep", "tp", None),
        P("ep", None, "tp"),
        P("tp", None),
        P("tp", None),
        P(None, "tp"),
        P("tp"),
    )
    out_specs = P("ep", "tp")
    return jax.shard_map(
        on_device, mesh=mesh, in_specs=in_specs, out_specs=out_specs, check_vma=False
    )
```

profile of v0, /device:TPU:29, one launch (start us, length us, event | category | flops | bytes accessed | tf_op | source)
XLA Modules:
  0.0 106.7 jit_solution(9834614439427043769)
XLA Ops:
  0.0 0.9 copy.24
  1.0 0.6 reduce-window.6
  1.6 0.2 slice_reduce_fusion
  2.1 0.7 multiply_add_fusion
  2.9 1.1 %fusion.12 = f32[24]{0:T(128)S(1)} fusion(bf16[24,4096]{1,0:T(8,128)(2,1)} %param.11), kind=kLoop, calls=%fused_computation.14 | loop fusion | flops 294888 | bytes 196704 | tf_op jit(solution)/shard_map/reduce_sum | solution.py:34
  4.0 1.5 %convolution_convert_fusion = bf16[160,4096]{1,0:T(8,128)(2,1)S(1)} fusion(pred[24,160]{1,0:T(8,128)(4,1)S(1)} %fusion.15, bf16[24,4096]{1,0:T(8,128)(2,1)} %param.11, f32[4096]{0:T(1024)} %param.12, f32[24]{0:T(128)S(1)} %add_rsqrt_fusion.1), kind=kOutput, calls=%fused_computation | convolution fusion | flops 32505856 | bytes 1527648 | tf_op jit(solution)/shard_map/dot_general | solution.py:53
  5.5 1.6 %reshape.45 = bf16[16,10,4096]{2,1,0:T(8,128)(2,1)} reshape(bf16[160,4096]{1,0:T(8,128)(2,1)S(1)} %convolution_convert_fusion) | data formatting | bytes 2621440 | tf_op jit(solution)/shard_map/reshape | solution.py:57
  7.1 52.9 %all_to_all.10 = bf16[16,10,4096]{2,1,0:T(8,128)(2,1)} all-to-all(bf16[16,10,4096]{2,1,0:T(8,128)(2,1)} %reshape.45), channel_id=1, replica_groups=mesh['ep'=16,'tp'=2] {'ep'}, dimensions={0} | all-to-all | bytes 2621440 | tf_op jit(solution)/shard_map/all_to_all | solution.py:56
  60.1 1.8 %reshape.46 = bf16[160,4096]{1,0:T(8,128)(2,1)S(1)} reshape(bf16[16,10,4096]{2,1,0:T(8,128)(2,1)} %all_to_all.10) | data formatting | bytes 2621440 | tf_op jit(solution)/shard_map/reshape | solution.py:63
  61.9 2.6 %fusion.3 = f32[160,256]{1,0:T(8,128)S(1)} fusion(bf16[160,4096]{1,0:T(8,128)(2,1)S(1)} %reshape.46, bf16[1,256,4096]{2,1,0:T(8,128)(2,1)} %param.15), kind=kOutput, calls=%fused_computation.6 | convolution fusion | flops 335544320 | bytes 3571712 | tf_op jit(solution)/shard_map/dot_general | solution.py:10
  64.5 0.9 fusion.8
  65.4 3.1 %all_gather.6 = bf16[160,512]{1,0:T(8,128)(2,1)S(1)} all-gather(bf16[160,256]{1,0:T(8,128)(2,1)S(1)} %fusion.8), channel_id=1, replica_groups=mesh['ep'=16,'tp'=2] {'tp'}, dimensions={1}, use_global_device_ids=true | all-gather | bytes 245760 | tf_op jit(solution)/shard_map/all_gather | solution.py:67
  68.4 0.5 convolution_convert_fusion.1
  69.0 1.2 %reshape.47 = bf16[16,10,2048]{2,1,0:T(8,128)(2,1)} reshape(bf16[160,2048]{1,0:T(8,128)(2,1)S(1)} %convolution_convert_fusion.1) | data formatting | bytes 1310720 | tf_op jit(solution)/shard_map/reshape | solution.py:75
  70.2 5.5 %all-to-all-start.1 = ((bf16[16,10,2048]{2,1,0:T(8,128)(2,1)}), bf16[16,10,2048]{2,1,0:T(8,128)(2,1)S(1)}, u32[]{:S(2)}, u32[]{:S(2)}) async-start(bf16[16,10,2048]{2,1,0:T(8,128)(2,1)} %reshape.47), calls=%async_computation.1 | async-start | bytes 2097152 | tf_op jit(solution)/shard_map/all_to_all | solution.py:74
  75.7 2.4 %fusion.19 = f32[24,256]{1,0:T(8,128)S(1)} fusion(bf16[256,4096]{1,0:T(8,128)(2,1)} %param.18, bf16[24,4096]{1,0:T(8,128)(2,1)S(1)} %copy-done.1, f32[4096]{0:T(1024)S(1)} %copy-done.4, f32[24]{0:T(128)S(1)} %add_rsqrt_fusion.1), kind=kOutput, calls=%fused_computation.35 | convolution fusion | flops 50724864 | bytes 2334816 | tf_op jit(solution)/shard_map/dot_general | solution.py:10
  78.1 0.7 fusion.11
  78.8 2.4 %all_gather.7 = bf16[24,512]{1,0:T(8,128)(2,1)S(1)} all-gather(bf16[24,256]{1,0:T(8,128)(2,1)S(1)} %fusion.11), channel_id=1, replica_groups=mesh['ep'=16,'tp'=2] {'tp'}, dimensions={1}, use_global_device_ids=true | all-gather | bytes 36864 | tf_op jit(solution)/shard_map/all_gather | solution.py:68
  81.3 0.4 fusion.22
  81.7 17.7 %all-to-all-done.1 = bf16[16,10,2048]{2,1,0:T(8,128)(2,1)S(1)} async-done(((bf16[16,10,2048]{2,1,0:T(8,128)(2,1)}), bf16[16,10,2048]{2,1,0:T(8,128)(2,1)S(1)}, u32[]{:S(2)}, u32[]{:S(2)}) %all-to-all-start.1) | async-done | bytes 655392 | tf_op jit(solution)/shard_map/all_to_all | solution.py:74
  99.4 1.1 reshape.48
  100.5 1.6 %multiply_reduce_fusion = (f32[24]{0:T(128)S(1)}, f32[24,2048]{1,0:T(8,128)S(1)}) fusion(f32[24,2048]{1,0:T(8,128)S(1)} %fusion.22, f32[24,160]{1,0:T(8,128)S(1)} %select_reduce_fusion, bf16[160,2048]{1,0:T(8,128)(2,1)} %reshape.48), kind=kOutput, calls=%fused_computation.18 | convolution fusion | flops 94519272 | bytes 1064032 | tf_op jit(solution)/shard_map/dot_general | solution.py:82
  102.0 3.9 %psum.7 = f32[24]{0:T(128)S(1)} all-reduce(f32[24]{0:T(128)S(1)} %get-tuple-element.5), channel_id=1, replica_groups=mesh['ep'=16,'tp'=2] {'tp'}, use_global_device_ids=true, to_apply=%region_7.8 | all-reduce | flops 24 | bytes 192 | tf_op jit(solution)/shard_map/psum | solution.py:84
  106.0 0.7 multiply_convert_fusion
  (29 shorter events, 0.7 us)
Async XLA Ops:
  0.0 68.4 %copy-start = (bf16[1,512,2048]{2,1,0:T(8,128)(2,1)S(1)}, bf16[1,512,2048]{2,1,0:T(8,128)(2,1)}, u32[]{:S(2)}) copy-start(bf16[1,512,2048]{2,1,0:T(8,128)(2,1)} %param.17) | copy-start | bytes 6291460
  61.9 2.6 %copy-start.7 = (bf16[1,256,4096]{2,1,0:T(8,128)(2,1)S(1)}, bf16[1,256,4096]{2,1,0:T(8,128)(2,1)}, u32[]{:S(2)}) copy-start(bf16[1,256,4096]{2,1,0:T(8,128)(2,1)} %param.16) | copy-start | bytes 6291460
  69.0 6.7 %copy-start.1 = (bf16[24,4096]{1,0:T(8,128)(2,1)S(1)}, bf16[24,4096]{1,0:T(8,128)(2,1)}, u32[]{:S(2)}) copy-start(bf16[24,4096]{1,0:T(8,128)(2,1)} %param.11) | copy-start | bytes 589828
  69.0 6.7 %copy-start.4 = (f32[4096]{0:T(1024)S(1)}, f32[4096]{0:T(1024)}, u32[]{:S(2)}) copy-start(f32[4096]{0:T(1024)} %param.12) | copy-start | bytes 49156
  70.2 29.2 %all-to-all-start.1 = ((bf16[16,10,2048]{2,1,0:T(8,128)(2,1)}), bf16[16,10,2048]{2,1,0:T(8,128)(2,1)S(1)}, u32[]{:S(2)}, u32[]{:S(2)}) async-start(bf16[16,10,2048]{2,1,0:T(8,128)(2,1)} %reshape.47), calls=%async_computation.1 | async-start | bytes 2097152 | tf_op jit(solution)/shard_map/all_to_all | solution.py:74
  75.7 2.5 %copy-start.2 = (bf16[256,4096]{1,0:T(8,128)(2,1)S(1)}, bf16[256,4096]{1,0:T(8,128)(2,1)}, u32[]{:S(2)}) copy-start(bf16[256,4096]{1,0:T(8,128)(2,1)} %param.19) | copy-start | bytes 6291460
  75.7 5.5 %copy-start.6 = (f32[24,6]{0,1:T(8,128)S(1)}, f32[24,6]{0,1:T(8,128)}, u32[]{:S(2)}) copy-start(f32[24,6]{0,1:T(8,128)} %param.14) | copy-start | bytes 1732
  75.7 5.6 %copy-start.3 = (bf16[512,2048]{1,0:T(8,128)(2,1)S(1)}, bf16[512,2048]{1,0:T(8,128)(2,1)}, u32[]{:S(2)}) copy-start(bf16[512,2048]{1,0:T(8,128)(2,1)} %param.20) | copy-start | bytes 6291460
  81.3 24.6 %copy-start.5 = (f32[2048]{0:T(1024)S(1)}, f32[2048]{0:T(1024)}, u32[]{:S(2)}) copy-start(f32[2048]{0:T(1024)} %param.21) | copy-start | bytes 24580
where the time goes:
time: 109 us; the launch traced here: 107 us
  blocking collectives  62.3 us (57%)
  waiting for transfers between devices  17.7 us (16%)
  matrix products  10.5 us (10%)
  local copies, waits for them, and re-layouts  7.07 us (6%)
  starting transfers between devices  5.46 us (5%)
  other arithmetic  3.46 us (3%)
    all_to_all x1, blocking collectives, on_device(): lax.all_to_all(buffer.reshape(experts, capacity, model_width), 'ep', spli...  52.9 us
    all_to_all x1, waiting for transfers between devices, on_device(): lax.all_to_all(outputs.reshape(experts, capacity, outputs.shape[1]), 'ep'...  17.7 us
    dot_general x4, matrix products, project(): lax.dot_general(rows, weight, (((1,), (1,)), ((), ())), preferred_element...  6.56 us
    all_to_all x1, starting transfers between devices, on_device(): lax.all_to_all(outputs.reshape(experts, capacity, outputs.shape[1]), 'ep'...  5.46 us
    psum x1, blocking collectives, on_device(): squares_sum = lax.psum(jnp.sum(combined * combined, axis=1), 'tp')  3.92 us
    all_gather x1, blocking collectives, on_device(): hidden_all = lax.all_gather(hidden, 'tp', axis=1, tiled=True)  3.06 us
    all_gather x1, blocking collectives, on_device(): shared_all = lax.all_gather(shared_hidden, 'tp', axis=1, tiled=True)  2.4 us
  transfers between devices with their start and end apart: 1, of which 1 were waited for; matrix products, arithmetic and copies ran while one was open for 3% of the time, Pallas kernels for 0%

commit v1 on v0

v1 whole, which is shorter than its diff:
```python
import functools

import jax
import jax.numpy as jnp
from jax import lax
from jax.experimental import pallas as pl
from jax.experimental.pallas import tpu as pltpu
from jax.sharding import PartitionSpec as P

EPS = 1e-06
MESH = pl.DeviceIdType.MESH
F32 = jnp.float32
BF16 = jnp.bfloat16


def dot_nt(a, b):
    return lax.dot_general(a, b, (((1,), (1,)), ((), ())), preferred_element_type=F32)


def dot_nn(a, b):
    return jnp.dot(a, b, preferred_element_type=F32)


def silu_mul(g, u):
    return g / (1.0 + jnp.exp(-g)) * u


def kernel(
    experts, cap, pad,
    tok, ing, routes, gates, eg, eu, ed, sg, su, sd, outg,
    o,
    vg, vu, vd, vsg, vsu, vsd,
    nrm, send, recv, acc_g, acc_u, sacc_g, sacc_u, hbuf, shbuf, outb, ret, comb, sq,
    wsem, lsem, dsend, drecv, fsend, frecv, rsend, rrecv, xsend, xrecv,
):
    me = lax.axis_index("ep")
    tp = lax.axis_index("tp")
    rows, width = tok.shape
    group = lax.axis_size("tp")
    half = width // group
    slots = experts * pad
    kc = min(512, half)

    loads = [
        pltpu.make_async_copy(src, dst, wsem.at[i])
        for i, (src, dst) in enumerate(
            ((sg, vsg), (su, vsu), (eg.at[0], vg), (eu.at[0], vu), (ed.at[0], vd), (sd, vsd))
        )
    ]
    for load in loads:
        load.start()

    ret[...] = jnp.zeros_like(ret)

    barrier = pltpu.get_barrier_semaphore()

    @pl.loop(1, experts)
    def _(k):
        pl.semaphore_signal(
            barrier, inc=1, device_id=(lax.rem(me + k, experts), tp), device_id_type=MESH
        )

    for q in range(1, group):
        pl.semaphore_signal(
            barrier, inc=1, device_id=(me, lax.rem(tp + q, group)), device_id_type=MESH
        )

    x = tok[...].astype(F32)
    scale = lax.rsqrt(jnp.mean(x * x, axis=1, keepdims=True) + EPS)
    for h in range(group):
        cols = slice(h * half, (h + 1) * half)
        nrm[h] = (tok[:, cols].astype(F32) * scale * ing[:, cols]).astype(BF16)

    expert_ids = lax.broadcasted_iota(jnp.int32, (rows, experts), 1)
    chosen = jnp.zeros((rows, experts), F32)
    weight = jnp.zeros((rows, experts), F32)
    for k in range(routes.shape[1]):
        hit = routes[:, k : k + 1] == expert_ids
        chosen = jnp.where(hit, 1.0, chosen)
        weight = jnp.where(hit, gates[:, k : k + 1], weight)
    chosen = chosen.astype(BF16)
    earlier = (
        lax.broadcasted_iota(jnp.int32, (rows, rows), 1)
        < lax.broadcasted_iota(jnp.int32, (rows, rows), 0)
    ).astype(F32).astype(BF16)
    rank = dot_nn(earlier, chosen).astype(BF16)
    slot_r = lax.broadcasted_iota(jnp.int32, (slots, experts), 0)
    spread_t = (
        slot_r // pad == lax.broadcasted_iota(jnp.int32, (slots, experts), 1)
    ).astype(F32).astype(BF16)
    place_r = (lax.broadcasted_iota(jnp.int32, (slots, rows), 0) % pad).astype(F32)
    placing = jnp.where(
        (dot_nt(spread_t, chosen) > 0.5) & (dot_nt(spread_t, rank) == place_r), 1.0, 0.0
    ).astype(BF16)
    for c in range(half // kc):
        cols = slice(c * kc, (c + 1) * kc)
        send[:, :, cols] = (
            dot_nn(placing, nrm[tp, :, cols]).astype(BF16).reshape(experts, pad, kc)
        )

    pl.semaphore_wait(barrier, experts - 1 + group - 1)

    def dispatch(dest, source):
        return pltpu.make_async_remote_copy(
            src_ref=send.at[dest],
            dst_ref=recv.at[tp, source],
            send_sem=dsend.at[dest],
            recv_sem=drecv.at[source],
            device_id=(dest, tp),
            device_id_type=MESH,
        )

    def forward(part, source, q):
        return pltpu.make_async_remote_copy(
            src_ref=recv.at[part, source],
            dst_ref=recv.at[part, source],
            send_sem=fsend.at[q, source],
            recv_sem=frecv.at[part, source],
            device_id=(me, lax.rem(tp + q, group)),
            device_id_type=MESH,
        )

    def give_back(dest, source):
        return pltpu.make_async_remote_copy(
            src_ref=outb.at[dest],
            dst_ref=ret.at[source],
            send_sem=rsend.at[dest],
            recv_sem=rrecv.at[source],
            device_id=(dest, tp),
            device_id_type=MESH,
        )

    def swap(ref, i, part, q):
        return pltpu.make_async_remote_copy(
            src_ref=ref.at[part],
            dst_ref=ref.at[part],
            send_sem=xsend.at[i, q],
            recv_sem=xrecv.at[i, part],
            device_id=(me, lax.rem(tp + q, group)),
            device_id_type=MESH,
        )

    def swap_start(ref, i):
        for q in range(1, group):
            swap(ref, i, tp, q).start()

    def swap_recv(ref, i):
        for q in range(1, group):
            swap(ref, i, lax.rem(tp + q, group), q).wait_recv()

    def swap_sent(ref, i):
        for q in range(1, group):
            swap(ref, i, tp, q).wait_send()

    def forward_start(source):
        for q in range(1, group):
            forward(tp, source, q).start()

    @pl.loop(1, experts)
    def _(k):
        dispatch(lax.rem(me + k, experts), me).start()

    own = pltpu.make_async_copy(
        send.at[me], recv.at[tp, me], lsem.at[0]
    )
    own.start()

    loads[0].wait()
    loads[1].wait()
    sacc_g[...] = jnp.zeros_like(sacc_g)
    sacc_u[...] = jnp.zeros_like(sacc_u)
    for h in range(group):

        @pl.loop(0, half // kc)
        def _(c):
            cols = pl.ds(pl.multiple_of(c * kc, kc), kc)
            wide = pl.ds(pl.multiple_of(h * half + c * kc, kc), kc)
            xs = nrm[h, :, cols]
            sacc_g[...] += dot_nt(xs, vsg[:, wide])
            sacc_u[...] += dot_nt(xs, vsu[:, wide])

    shbuf[tp] = silu_mul(sacc_g[...], sacc_u[...]).astype(BF16)
    swap_start(shbuf, 0)

    own.wait()
    forward_start(me)

    @pl.loop(1, experts)
    def _(k):
        source = lax.rem(me + experts - k, experts)
        dispatch(source, source).wait_recv()
        forward_start(source)

    loads[2].wait()
    loads[3].wait()
    acc_g[...] = jnp.zeros_like(acc_g)
    acc_u[...] = jnp.zeros_like(acc_u)

    def project_part(part):
        @pl.loop(0, half // kc)
        def _(c):
            cols = pl.ds(pl.multiple_of(c * kc, kc), kc)
            wide = pl.ds(pl.multiple_of(part * half + c * kc, kc), kc)
            xs = recv[part, :, :, cols].reshape(slots, kc)
            acc_g[...] += dot_nt(xs, vg[:, wide])
            acc_u[...] += dot_nt(xs, vu[:, wide])

    project_part(tp)

    for q in range(1, group):
        part = lax.rem(tp + q, group)

        @pl.loop(0, experts)
        def _(k):
            forward(part, lax.rem(me + experts - k, experts), q).wait_recv()

        project_part(part)

    hbuf[tp] = silu_mul(acc_g[...], acc_u[...]).astype(BF16)
    swap_start(hbuf, 1)
    loads[4].wait()
    swap_recv(hbuf, 1)

    def down(hidden, weights, cols):
        depth = weights.shape[0] // group
        return sum(
            dot_nn(hidden[p], weights[p * depth : (p + 1) * depth, cols]) for p in range(group)
        )

    for c in range(half // kc):
        cols = slice(c * kc, (c + 1) * kc)
        outb[:, :, cols] = (
            down(hbuf, vd, cols).astype(BF16).reshape(experts, pad, kc)
        )

    @pl.loop(1, experts)
    def _(k):
        give_back(lax.rem(me + k, experts), me).start()

    own_back = pltpu.make_async_copy(
        outb.at[me], ret.at[me], lsem.at[1]
    )
    own_back.start()

    loads[5].wait()
    swap_recv(shbuf, 0)
    for c in range(half // kc):
        cols = slice(c * kc, (c + 1) * kc)
        comb[:, cols] = down(shbuf, vsd, cols)
    spread = (
        lax.broadcasted_iota(jnp.int32, (experts, slots), 1) // pad
        == lax.broadcasted_iota(jnp.int32, (experts, slots), 0)
    ).astype(F32).astype(BF16)
    place = (lax.broadcasted_iota(jnp.int32, (rows, slots), 1) % pad).astype(F32)
    taken = (dot_nn(chosen, spread) > 0.5) & (dot_nn(rank, spread) == place)
    coarse = weight.astype(BF16)
    fine = (weight - coarse.astype(F32)).astype(BF16)
    mix_coarse = jnp.where(taken, dot_nn(coarse, spread), 0.0).astype(BF16)
    mix_fine = jnp.where(taken, dot_nn(fine, spread), 0.0).astype(BF16)

    own_back.wait()

    @pl.loop(1, experts)
    def _(k):
        source = lax.rem(me + experts - k, experts)
        give_back(source, source).wait_recv()

    total = jnp.zeros((rows, 1), F32)
    for c in range(half // kc):
        cols = slice(c * kc, (c + 1) * kc)
        back = ret[:, :, cols].reshape(slots, kc)
        part = comb[:, cols] + dot_nn(mix_coarse, back) + dot_nn(mix_fine, back)
        comb[:, cols] = part
        total = total + jnp.sum(part * part, axis=1, keepdims=True)
    sq[tp] = jnp.broadcast_to(total, sq.shape[1:])
    swap_start(sq, 2)

    @pl.loop(1, experts)
    def _(k):
        dest = lax.rem(me + k, experts)
        dispatch(dest, me).wait_send()
        give_back(dest, me).wait_send()

    @pl.loop(0, experts)
    def _(k):
        for q in range(1, group):
            forward(tp, k, q).wait_send()

    swap_sent(shbuf, 0)
    swap_sent(hbuf, 1)
    swap_recv(sq, 2)
    norm = lax.rsqrt(sum(sq[p] for p in range(group))[:, :1] / width + EPS)
    o[...] = (comb[...] * norm * outg[...]).astype(BF16)
    swap_sent(sq, 2)


def on_device(experts, tokens, in_gain, routes, gates, eg, eu, ed, sg, su, sd, out_gain):
    rows, width = tokens.shape
    group = lax.axis_size("tp")
    half = width // group
    cap = min(rows, (rows * routes.shape[1] + experts - 1) // experts + 1)
    pad = -(-cap // 16) * 16
    slots = experts * pad
    hid, shid = eg.shape[1], sg.shape[0]
    vmem = pl.BlockSpec(memory_space=pltpu.VMEM)
    hbm = pl.BlockSpec(memory_space=pl.ANY)
    dma = pltpu.SemaphoreType.DMA
    return pl.pallas_call(
        functools.partial(kernel, experts, cap, pad),
        out_shape=jax.ShapeDtypeStruct((rows, half), BF16),
        in_specs=[vmem] * 4 + [hbm] * 6 + [vmem],
        out_specs=vmem,
        scratch_shapes=[
            pltpu.VMEM(eg.shape[1:], BF16),
            pltpu.VMEM(eu.shape[1:], BF16),
            pltpu.VMEM(ed.shape[1:], BF16),
            pltpu.VMEM(sg.shape, BF16),
            pltpu.VMEM(su.shape, BF16),
            pltpu.VMEM(sd.shape, BF16),
            pltpu.VMEM((group, rows, half), BF16),
            pltpu.VMEM((experts, pad, half), BF16),
            pltpu.VMEM((group, experts, pad, half), BF16),
            pltpu.VMEM((slots, hid), F32),
            pltpu.VMEM((slots, hid), F32),
            pltpu.VMEM((rows, shid), F32),
            pltpu.VMEM((rows, shid), F32),
            pltpu.VMEM((group, slots, hid), BF16),
            pltpu.VMEM((group, rows, shid), BF16),
            pltpu.VMEM((experts, pad, half), BF16),
            pltpu.VMEM((experts, pad, half), BF16),
            pltpu.VMEM((rows, half), F32),
            pltpu.VMEM((group, rows, 128), F32),
            dma((6,)),
            dma((2,)),
            dma((experts,)),
            dma((experts,)),
            dma((group, experts)),
            dma((group, experts)),
            dma((experts,)),
            dma((experts,)),
            dma((3, group)),
            dma((3, group)),
        ],
        compiler_params=pltpu.CompilerParams(
            collective_id=0, has_side_effects=True, vmem_limit_bytes=60 * 1024 * 1024
        ),
    )(
        tokens, in_gain.reshape(1, width), routes, gates, eg, eu, ed, sg, su, sd,
        out_gain.reshape(1, half),
    )


def solution(mesh):
    in_specs = (
        P("ep", None),
        P(),
        P("ep", None),
        P("ep", None),
        P("ep", "tp", None),
        P("ep", "tp", None),
        P("ep", None, "tp"),
        P("tp", None),
        P("tp", None),
        P(None, "tp"),
        P("tp"),
    )
    return jax.shard_map(
        functools.partial(on_device, mesh.shape["ep"]),
        mesh=mesh,
        in_specs=in_specs,
        out_specs=P("ep", "tp"),
        check_vma=False,
    )
```

time: 109 us -> 67.8 us (0.62); the launches traced: 107 us -> 67.1 us
  Pallas kernels: 0 us -> 62.8 us
  blocking collectives: 62.3 us -> 0 us
  waiting for transfers between devices: 17.7 us -> 0 us
  matrix products: 10.5 us -> 0 us
  starting transfers between devices: 5.46 us -> 0 us
  other arithmetic: 3.46 us -> 0 us
  local copies, waits for them, and re-layouts: 7.07 us -> 4.26 us
    pallas_call x0 -> x1, Pallas kernels: none -> 62.8 us  [on_device(): pl.pallas_call(functools.partial(kernel, experts, cap, pad), out_shape=ja...]
    all_to_all x1 -> x0, blocking collectives: 52.9 us -> none  [on_device(): lax.all_to_all(buffer.reshape(experts, capacity, model_width), 'ep', spli...]
    all_to_all x1 -> x0, waiting for transfers between devices: 17.7 us -> none  [on_device(): lax.all_to_all(outputs.reshape(experts, capacity, outputs.shape[1]), 'ep'...]
    dot_general x8 -> x0, matrix products: 10.5 us -> none  [the longest x4 6.56 us: project(): lax.dot_general(rows, weight, (((1,), (1,)), ((), ())), preferred_element...]
    reshape x4 -> x0, local copies, waits for them, and re-layouts: 5.64 us -> none  [the longest x1 1.79 us: on_device(): token_rows = arrived.reshape(experts * capacity, model_width)]
    all_to_all x1 -> x0, starting transfers between devices: 5.46 us -> none  [on_device(): lax.all_to_all(outputs.reshape(experts, capacity, outputs.shape[1]), 'ep'...]
    all_gather x2 -> x0, blocking collectives: 5.45 us -> none  [the longest x1 3.06 us: on_device(): hidden_all = lax.all_gather(hidden, 'tp', axis=1, tiled=True)]
    psum x1 -> x0, blocking collectives: 3.92 us -> none  [on_device(): squares_sum = lax.psum(jnp.sum(combined * combined, axis=1), 'tp')]
  transfers between devices with their start and end apart: 1 -> 0, of which waited for: 1 -> 0; matrix products, arithmetic and copies ran while one was open for 3% -> 0% of each run, Pallas kernels for 0% -> 0%
where the time goes in v1:
time: 67.8 us; the launch traced here: 67.1 us
  Pallas kernels  62.8 us (93%)
  local copies, waits for them, and re-layouts  4.26 us (6%)
    pallas_call x1, Pallas kernels, on_device(): pl.pallas_call(functools.partial(kernel, experts, cap, pad), out_shape=ja...  62.8 us
    unnamed x3, local copies, waits for them, and re-layouts  4.26 us

profile of v1, /device:TPU:29, one launch (start us, length us, event | category | flops | bytes accessed | tf_op | source)
XLA Modules:
  0.0 67.1 jit_solution(10708352797541732767)
XLA Ops:
  0.0 1.4 %copy.12.routes = s32[24,6]{1,0:T(8,128)} copy(s32[24,6]{0,1:T(8,128)} %param.13) | data formatting | bytes 1152 | tf_op args[2]
  1.4 1.4 %copy.13.gates = f32[24,6]{1,0:T(8,128)} copy(f32[24,6]{0,1:T(8,128)} %param.14) | data formatting | bytes 1152 | tf_op args[3]
  2.7 62.8 %shard_map.109 = bf16[24,2048]{1,0:T(8,128)(2,1)} custom-call(bf16[24,4096]{1,0:T(8,128)(2,1)} %tok.1, f32[1,4096]{1,0:T(1,128)} %bitcast.2, s32[24,6]{1,0:T(8,128)} %copy.12.routes, f32[24,6]{1,0:T(8,128)} %copy.13.gates, bf16[1,256,4096]{2,1,0:T(8,128)(2,1)} %eg.1, bf16[1,256,4096]{2,1,0:T(8,128)(2,1)} %eu.1, bf16[1,512,2048]{2,1,0:T(8,128)(2,1)} %ed.1, ...), custom_call_target="tpu_custom_call" | custom-call | tf_op jit(solution)/shard_map/pallas_call | solution.py:308
  65.6 1.5 %copy.15 = bf16[24,2048]{1,0:T(8,128)(2,1)} copy(bf16[24,2048]{1,0:T(8,128)(2,1)} %shard_map.109) | data formatting | bytes 196608

commit v2 on v1

--- a/solution.py
+++ b/solution.py
@@ -26,7 +26,7 @@
 
 
 def kernel(
-    experts, cap, pad,
+    experts, fulls, rest,
     tok, ing, routes, gates, eg, eu, ed, sg, su, sd, outg,
     o,
     vg, vu, vd, vsg, vsu, vsd,
@@ -38,8 +38,10 @@
     rows, width = tok.shape
     group = lax.axis_size("tp")
     half = width // group
-    slots = experts * pad
-    kc = min(512, half)
+    slots = experts * 8
+    folds = 8 // rest if rest else 1
+    kc = half // folds if rest else min(512, half)
+    blocks = fulls + (1 if rest else 0)
 
     loads = [
         pltpu.make_async_copy(src, dst, wsem.at[i])
@@ -49,8 +51,6 @@
     ]
     for load in loads:
         load.start()
-
-    ret[...] = jnp.zeros_like(ret)
 
     barrier = pltpu.get_barrier_semaphore()
 
@@ -71,39 +71,60 @@
         cols = slice(h * half, (h + 1) * half)
         nrm[h] = (tok[:, cols].astype(F32) * scale * ing[:, cols]).astype(BF16)
 
-    expert_ids = lax.broadcasted_iota(jnp.int32, (rows, experts), 1)
-    chosen = jnp.zeros((rows, experts), F32)
-    weight = jnp.zeros((rows, experts), F32)
-    for k in range(routes.shape[1]):
-        hit = routes[:, k : k + 1] == expert_ids
-        chosen = jnp.where(hit, 1.0, chosen)
-        weight = jnp.where(hit, gates[:, k : k + 1], weight)
-    chosen = chosen.astype(BF16)
-    earlier = (
-        lax.broadcasted_iota(jnp.int32, (rows, rows), 1)
-        < lax.broadcasted_iota(jnp.int32, (rows, rows), 0)
+    expert_ids = lax.broadcasted_iota(jnp.int32, (experts, rows), 0)
+    chosen_t = jnp.zeros((experts, rows), F32)
+    weight_t = jnp.zeros((experts, rows), F32)
+    for k in range(routes.shape[0]):
+        hit = routes[k : k + 1, :] == expert_ids
+        chosen_t = jnp.where(hit, 1.0, chosen_t)
+        weight_t = jnp.where(hit, gates[k : k + 1, :], weight_t)
+    chosen_t = chosen_t.astype(BF16)
+    token_r = lax.broadcasted_iota(jnp.int32, (rows, rows), 0)
+    token_c = lax.broadcasted_iota(jnp.int32, (rows, rows), 1)
+    earlier = (token_r < token_c).astype(F32).astype(BF16)
+    rank_t = dot_nn(chosen_t, earlier).astype(BF16)
+
+    def places(slot):
+        row = slot % 8
+        listed = [((8 * i + row).astype(F32), None) for i in range(fulls)]
+        if rest:
+            listed.append(((8 * fulls + row % rest).astype(F32), row // rest))
+        return listed
+
+    spread_t = (
+        lax.broadcasted_iota(jnp.int32, (slots, experts), 0) // 8
+        == lax.broadcasted_iota(jnp.int32, (slots, experts), 1)
     ).astype(F32).astype(BF16)
-    rank = dot_nn(earlier, chosen).astype(BF16)
-    slot_r = lax.broadcasted_iota(jnp.int32, (slots, experts), 0)
-    spread_t = (
-        slot_r // pad == lax.broadcasted_iota(jnp.int32, (slots, experts), 1)
-    ).astype(F32).astype(BF16)
-    place_r = (lax.broadcasted_iota(jnp.int32, (slots, rows), 0) % pad).astype(F32)
-    placing = jnp.where(
-        (dot_nt(spread_t, chosen) > 0.5) & (dot_nt(spread_t, rank) == place_r), 1.0, 0.0
-    ).astype(BF16)
-    for c in range(half // kc):
-        cols = slice(c * kc, (c + 1) * kc)
-        send[:, :, cols] = (
-            dot_nn(placing, nrm[tp, :, cols]).astype(BF16).reshape(experts, pad, kc)
-        )
+    named_t = dot_nn(spread_t, chosen_t) > 0.5
+    ranks_t = dot_nn(spread_t, rank_t)
+    for i, (place, piece) in enumerate(
+        places(lax.broadcasted_iota(jnp.int32, (slots, rows), 0))
+    ):
+        here = jnp.where(named_t & (ranks_t == place), 1.0, 0.0)
+        if piece is None:
+            here = here.astype(BF16)
+            for c in range(half // kc):
+                send[:, i * half + c * kc : i * half + (c + 1) * kc] = dot_nn(
+                    here, nrm[tp, :, c * kc : (c + 1) * kc]
+                ).astype(BF16)
+        else:
+            send[:, i * half : i * half + kc] = sum(
+                dot_nn(
+                    jnp.where(piece == c, here, 0.0).astype(BF16),
+                    nrm[tp, :, c * kc : (c + 1) * kc],
+                )
+                for c in range(folds)
+            ).astype(BF16)
+
+    def own_rows(expert):
+        return pl.ds(pl.multiple_of(expert * 8, 8), 8)
 
     pl.semaphore_wait(barrier, experts - 1 + group - 1)
 
     def dispatch(dest, source):
         return pltpu.make_async_remote_copy(
-            src_ref=send.at[dest],
-            dst_ref=recv.at[tp, source],
+            src_ref=send.at[own_rows(dest)],
+            dst_ref=recv.at[tp, own_rows(source)],
             send_sem=dsend.at[dest],
             recv_sem=drecv.at[source],
             device_id=(dest, tp),
@@ -112,8 +133,8 @@
 
     def forward(part, source, q):
         return pltpu.make_async_remote_copy(
-            src_ref=recv.at[part, source],
-            dst_ref=recv.at[part, source],
+            src_ref=recv.at[part, own_rows(source)],
+            dst_ref=recv.at[part, own_rows(source)],
             send_sem=fsend.at[q, source],
             recv_sem=frecv.at[part, source],
             device_id=(me, lax.rem(tp + q, group)),
@@ -122,8 +143,8 @@
 
     def give_back(dest, source):
         return pltpu.make_async_remote_copy(
-            src_ref=outb.at[dest],
-            dst_ref=ret.at[source],
+            src_ref=outb.at[own_rows(dest)],
+            dst_ref=ret.at[own_rows(source)],
             send_sem=rsend.at[dest],
             recv_sem=rrecv.at[source],
             device_id=(dest, tp),
@@ -161,7 +182,7 @@
         dispatch(lax.rem(me + k, experts), me).start()
 
     own = pltpu.make_async_copy(
-        send.at[me], recv.at[tp, me], lsem.at[0]
+        send.at[own_rows(me)], recv.at[tp, own_rows(me)], lsem.at[0]
     )
     own.start()
 
@@ -196,12 +217,22 @@
     acc_g[...] = jnp.zeros_like(acc_g)
     acc_u[...] = jnp.zeros_like(acc_u)
 
+    if rest:
+        row_piece = lax.broadcasted_iota(jnp.int32, (slots, kc), 0) % 8 // rest
+
     def project_part(part):
         @pl.loop(0, half // kc)
         def _(c):
             cols = pl.ds(pl.multiple_of(c * kc, kc), kc)
             wide = pl.ds(pl.multiple_of(part * half + c * kc, kc), kc)
-            xs = recv[part, :, :, cols].reshape(slots, kc)
+            pieces = [
+                recv[part, :, pl.ds(pl.multiple_of(i * half + c * kc, kc), kc)]
+                for i in range(fulls)
+            ]
+            if rest:
+                last = recv[part, :, fulls * half : fulls * half + kc]
+                pieces.append(jnp.where(row_piece == c, last, jnp.zeros_like(last)))
+            xs = jnp.concatenate(pieces, axis=0)
             acc_g[...] += dot_nt(xs, vg[:, wide])
             acc_u[...] += dot_nt(xs, vu[:, wide])
 
@@ -216,7 +247,20 @@
 
         project_part(part)
 
-    hbuf[tp] = silu_mul(acc_g[...], acc_u[...]).astype(BF16)
+    for i in range(blocks):
+        block = slice(i * slots, (i + 1) * slots)
+        g, u = acc_g[block], acc_u[block]
+        if i == fulls:
+            g = g.reshape(experts, 8, -1)
+            u = u.reshape(experts, 8, -1)
+            shift = rest
+            while shift < 8:
+                g = g + pltpu.roll(g, shift, 1)
+                u = u + pltpu.roll(u, shift, 1)
+                shift *= 2
+            g = g.reshape(slots, -1)
+            u = u.reshape(slots, -1)
+        hbuf[tp, block] = silu_mul(g, u).astype(BF16)
     swap_start(hbuf, 1)
     loads[4].wait()
     swap_recv(hbuf, 1)
@@ -229,16 +273,23 @@
 
     for c in range(half // kc):
         cols = slice(c * kc, (c + 1) * kc)
-        outb[:, :, cols] = (
-            down(hbuf, vd, cols).astype(BF16).reshape(experts, pad, kc)
-        )
+        made = down(hbuf, vd, cols)
+        for i in range(fulls):
+            outb[:, i * half + c * kc : i * half + (c + 1) * kc] = made[
+                i * slots : (i + 1) * slots
+            ].astype(BF16)
+        if rest:
+            fresh = made[fulls * slots :]
+            last = fresh if c == 0 else jnp.where(row_piece == c, fresh, last)
+    if rest:
+        outb[:, fulls * half :] = last.astype(BF16)
 
     @pl.loop(1, experts)
     def _(k):
         give_back(lax.rem(me + k, experts), me).start()
 
     own_back = pltpu.make_async_copy(
-        outb.at[me], ret.at[me], lsem.at[1]
+        outb.at[own_rows(me)], ret.at[own_rows(me)], lsem.at[1]
     )
     own_back.start()
 
@@ -248,15 +299,19 @@
         cols = slice(c * kc, (c + 1) * kc)
         comb[:, cols] = down(shbuf, vsd, cols)
     spread = (
-        lax.broadcasted_iota(jnp.int32, (experts, slots), 1) // pad
+        lax.broadcasted_iota(jnp.int32, (experts, slots), 1) // 8
         == lax.broadcasted_iota(jnp.int32, (experts, slots), 0)
     ).astype(F32).astype(BF16)
-    place = (lax.broadcasted_iota(jnp.int32, (rows, slots), 1) % pad).astype(F32)
-    taken = (dot_nn(chosen, spread) > 0.5) & (dot_nn(rank, spread) == place)
-    coarse = weight.astype(BF16)
-    fine = (weight - coarse.astype(F32)).astype(BF16)
-    mix_coarse = jnp.where(taken, dot_nn(coarse, spread), 0.0).astype(BF16)
-    mix_fine = jnp.where(taken, dot_nn(fine, spread), 0.0).astype(BF16)
+    eye = (token_r == token_c).astype(F32).astype(BF16)
+    coarse_t = weight_t.astype(BF16)
+    fine_t = (weight_t - coarse_t.astype(F32)).astype(BF16)
+    named, ranks, coarse, fine = [
+        dot_nn(dot_nt(eye, t).astype(BF16), spread) for t in (chosen_t, rank_t, coarse_t, fine_t)
+    ]
+    mixing = []
+    for place, piece in places(lax.broadcasted_iota(jnp.int32, (rows, slots), 1)):
+        taken = (named > 0.5) & (ranks == place)
+        mixing.append((taken, piece))
 
     own_back.wait()
 
@@ -268,8 +323,15 @@
     total = jnp.zeros((rows, 1), F32)
     for c in range(half // kc):
         cols = slice(c * kc, (c + 1) * kc)
-        back = ret[:, :, cols].reshape(slots, kc)
-        part = comb[:, cols] + dot_nn(mix_coarse, back) + dot_nn(mix_fine, back)
+        part = comb[:, cols]
+        for i, (taken, piece) in enumerate(mixing):
+            if piece is None:
+                back = ret[:, i * half + c * kc : i * half + (c + 1) * kc]
+            else:
+                back = ret[:, i * half : i * half + kc]
+                taken = taken & (piece == c)
+            part += dot_nn(jnp.where(taken, coarse, 0.0).astype(BF16), back)
+            part += dot_nn(jnp.where(taken, fine, 0.0).astype(BF16), back)
         comb[:, cols] = part
         total = total + jnp.sum(part * part, axis=1, keepdims=True)
     sq[tp] = jnp.broadcast_to(total, sq.shape[1:])
@@ -299,14 +361,22 @@
     group = lax.axis_size("tp")
     half = width // group
     cap = min(rows, (rows * routes.shape[1] + experts - 1) // experts + 1)
-    pad = -(-cap // 16) * 16
-    slots = experts * pad
+    fulls, rest = cap // 8, cap % 8
+    while rest & (rest - 1):
+        rest += 1
+    if rest and half * rest // 8 % 128:
+        rest = 8
+    if rest == 8:
+        fulls, rest = fulls + 1, 0
+    slots = experts * 8
+    blocks = fulls + (1 if rest else 0)
+    packed = fulls * half + half * rest // 8
     hid, shid = eg.shape[1], sg.shape[0]
     vmem = pl.BlockSpec(memory_space=pltpu.VMEM)
     hbm = pl.BlockSpec(memory_space=pl.ANY)
     dma = pltpu.SemaphoreType.DMA
     return pl.pallas_call(
-        functools.partial(kernel, experts, cap, pad),
+        functools.partial(kernel, experts, fulls, rest),
         out_shape=jax.ShapeDtypeStruct((rows, half), BF16),
         in_specs=[vmem] * 4 + [hbm] * 6 + [vmem],
         out_specs=vmem,
@@ -318,16 +388,16 @@
             pltpu.VMEM(su.shape, BF16),
             pltpu.VMEM(sd.shape, BF16),
             pltpu.VMEM((group, rows, half), BF16),
-            pltpu.VMEM((experts, pad, half), BF16),
-            pltpu.VMEM((group, experts, pad, half), BF16),
-            pltpu.VMEM((slots, hid), F32),
-            pltpu.VMEM((slots, hid), F32),
+            pltpu.VMEM((slots, packed), BF16),
+            pltpu.VMEM((group, slots, packed), BF16),
+            pltpu.VMEM((blocks * slots, hid), F32),
+            pltpu.VMEM((blocks * slots, hid), F32),
             pltpu.VMEM((rows, shid), F32),
             pltpu.VMEM((rows, shid), F32),
-            pltpu.VMEM((group, slots, hid), BF16),
+            pltpu.VMEM((group, blocks * slots, hid), BF16),
             pltpu.VMEM((group, rows, shid), BF16),
-            pltpu.VMEM((experts, pad, half), BF16),
-            pltpu.VMEM((experts, pad, half), BF16),
+            pltpu.VMEM((slots, packed), BF16),
+            pltpu.VMEM((slots, packed), BF16),
             pltpu.VMEM((rows, half), F32),
             pltpu.VMEM((group, rows, 128), F32),
             dma((6,)),
@@ -345,7 +415,7 @@
             collective_id=0, has_side_effects=True, vmem_limit_bytes=60 * 1024 * 1024
         ),
     )(
-        tokens, in_gain.reshape(1, width), routes, gates, eg, eu, ed, sg, su, sd,
+        tokens, in_gain.reshape(1, width), routes.T, gates.T, eg, eu, ed, sg, su, sd,
         out_gain.reshape(1, half),
     )
 

time: 67.8 us -> 46.5 us (0.69)
  Pallas kernels: 62.8 us -> 44.8 us
  local copies, waits for them, and re-layouts: 4.26 us -> 1.54 us
    pallas_call x1, Pallas kernels: 62.8 us -> 44.8 us  [on_device(): pl.pallas_call(functools.partial(kernel, experts, fulls, rest), out_shape...]
    unnamed x3 -> x1, local copies, waits for them, and re-layouts: 4.26 us -> 1.54 us
where the time goes in v2:
time: 46.5 us; the launch traced here: 46.3 us
  Pallas kernels  44.8 us (96%)
  local copies, waits for them, and re-layouts  1.54 us (3%)
    pallas_call x1, Pallas kernels, on_device(): pl.pallas_call(functools.partial(kernel, experts, fulls, rest), out_shape...  44.8 us
    unnamed x1, local copies, waits for them, and re-layouts  1.54 us

profile of v2, /device:TPU:29, one launch (start us, length us, event | category | flops | bytes accessed | tf_op | source)
XLA Modules:
  0.0 46.3 jit_solution(10777040736970415554)
XLA Ops:
  0.0 44.8 %shard_map.109 = bf16[24,2048]{1,0:T(8,128)(2,1)} custom-call(bf16[24,4096]{1,0:T(8,128)(2,1)} %tok.1, f32[1,4096]{1,0:T(1,128)} %bitcast.4, s32[6,24]{1,0:T(8,128)} %bitcast.6, f32[6,24]{1,0:T(8,128)} %bitcast.7, bf16[1,256,4096]{2,1,0:T(8,128)(2,1)} %eg.1, bf16[1,256,4096]{2,1,0:T(8,128)(2,1)} %eu.1, bf16[1,512,2048]{2,1,0:T(8,128)(2,1)} %ed.1, ...), custom_call_target="tpu_custom_call" | custom-call | tf_op jit(solution)/shard_map/pallas_call | solution.py:378
  44.8 1.5 %copy.13 = bf16[24,2048]{1,0:T(8,128)(2,1)} copy(bf16[24,2048]{1,0:T(8,128)(2,1)} %shard_map.109) | data formatting | bytes 196608

commit v3 on v2

--- a/solution.py
+++ b/solution.py
@@ -67,9 +67,12 @@
 
     x = tok[...].astype(F32)
     scale = lax.rsqrt(jnp.mean(x * x, axis=1, keepdims=True) + EPS)
-    for h in range(group):
-        cols = slice(h * half, (h + 1) * half)
-        nrm[h] = (tok[:, cols].astype(F32) * scale * ing[:, cols]).astype(BF16)
+
+    def normalize(part):
+        cols = pl.ds(pl.multiple_of(part * half, half), half)
+        nrm[part] = (tok[:, cols].astype(F32) * scale * ing[:, cols]).astype(BF16)
+
+    normalize(tp)
 
     expert_ids = lax.broadcasted_iota(jnp.int32, (experts, rows), 0)
     chosen_t = jnp.zeros((experts, rows), F32)
@@ -186,6 +189,8 @@
     )
     own.start()
 
+    for q in range(1, group):
+        normalize(lax.rem(tp + q, group))
     loads[0].wait()
     loads[1].wait()
     sacc_g[...] = jnp.zeros_like(sacc_g)
@@ -330,8 +335,11 @@
             else:
                 back = ret[:, i * half : i * half + kc]
                 taken = taken & (piece == c)
-            part += dot_nn(jnp.where(taken, coarse, 0.0).astype(BF16), back)
-            part += dot_nn(jnp.where(taken, fine, 0.0).astype(BF16), back)
+            both = jnp.concatenate(
+                [jnp.where(taken, coarse, 0.0), jnp.where(taken, fine, 0.0)], axis=0
+            )
+            mixed = dot_nn(both.astype(BF16), back)
+            part += mixed[:rows] + mixed[rows:]
         comb[:, cols] = part
         total = total + jnp.sum(part * part, axis=1, keepdims=True)
     sq[tp] = jnp.broadcast_to(total, sq.shape[1:])

time: 46.5 us -> 46.4 us (level)
  no operation moved by 1% of the time
where the time goes in v3:
time: 46.4 us; the launch traced here: 46.2 us
  Pallas kernels  44.7 us (96%)
  local copies, waits for them, and re-layouts  1.54 us (3%)
    pallas_call x1, Pallas kernels, on_device(): pl.pallas_call(functools.partial(kernel, experts, fulls, rest), out_shape...  44.7 us
    unnamed x1, local copies, waits for them, and re-layouts  1.54 us

profile of v3, /device:TPU:29, one launch (start us, length us, event | category | flops | bytes accessed | tf_op | source)
XLA Modules:
  0.0 46.2 jit_solution(8303957775887837785)
XLA Ops:
  0.0 44.7 %shard_map.109 = bf16[24,2048]{1,0:T(8,128)(2,1)} custom-call(bf16[24,4096]{1,0:T(8,128)(2,1)} %tok.1, f32[1,4096]{1,0:T(1,128)} %bitcast.4, s32[6,24]{1,0:T(8,128)} %bitcast.6, f32[6,24]{1,0:T(8,128)} %bitcast.7, bf16[1,256,4096]{2,1,0:T(8,128)(2,1)} %eg.1, bf16[1,256,4096]{2,1,0:T(8,128)(2,1)} %eu.1, bf16[1,512,2048]{2,1,0:T(8,128)(2,1)} %ed.1, ...), custom_call_target="tpu_custom_call" | custom-call | tf_op jit(solution)/shard_map/pallas_call | solution.py:386
  44.7 1.5 %copy.13 = bf16[24,2048]{1,0:T(8,128)(2,1)} copy(bf16[24,2048]{1,0:T(8,128)(2,1)} %shard_map.109) | data formatting | bytes 196608
